TPU v7x, 32 devices: a whole 2x2x4 slice. The times are simulated.
32 devices in a mesh: grp: 2 (over y), dp: 2 (over x), kv: 4 (over z), tp: 2 (over core).
Axes of the slice: x: 2, y: 2, z: 4, core: 2. Of those that a mesh axis runs over, the one named last changes fastest.
Arguments:
- tokens: bfloat16 [4, 1536, 2048], P(('grp', 'dp'), 'kv'), parts along dimension 0, may hold values from -14 to 14
- query_weight: bfloat16 [2048, 1024], P('kv', 'tp'), may hold values from -0.1875 to 0.1875
- key_weight: bfloat16 [2048, 512], P('kv', 'tp'), may hold values from -0.1875 to 0.1875
- value_weight: bfloat16 [2048, 512], P('kv', 'tp'), may hold values from -0.125 to 0.125
- output_weight: bfloat16 [1024, 2048], P('tp', 'kv'), may hold values from -3.59375 to 3.59375
- block_choice: int32 [4, 24, 16], P(('grp', 'dp'), 'kv'), parts along dimension 0, may hold values from -1 to 23, as said below
Outputs:
- attention: bfloat16 [4, 1536, 2048], P(('grp', 'dp'), 'kv', 'tp'), parts along dimension 0
There are 2 independent parts, one for each index of `grp`. A program takes and returns all parts, laid end to end along the dimension named above; an argument that names none is the same for every part. Nothing has to cross between parts.
Inputs may be any that keep to these rules, and one draw needn't show every extreme that they name: `block_choice`: row i of a sequence names distinct key blocks below i, the named ones first and -1 in the slots after them. Split the rows into aligned groups of 6 (the query blocks that share one index of kv, whose key blocks are the same 6 blocks): the rows of one group name at most 4 distinct blocks among those of any other group, and every row of a group names all of exactly 4 blocks of the group just before it.
All inputs are finite; a program needn't handle non-finite values.
Results may differ from a plain program's by a relative error of at most 0.012.
Values may be sent and summed in bfloat16 or wider, within the bound.
A program may use at most 64 MiB of HBM per device.

v0:
```python
import jax
import jax.numpy as jnp
from jax import lax
from jax.sharding import PartitionSpec as P

HEAD = 128
BLOCK = 64
NSEL = 16


THETA = 10000.0
NEGATIVE = -1e30


def rotate(field_rows, positions):
    half_width = HEAD // 2
    inverse = THETA ** (-jnp.arange(half_width, dtype=jnp.float32) / half_width)
    angles = positions.astype(jnp.float32)[:, None] * inverse[None, :]
    cosine = jnp.cos(angles)[:, None, :]
    sine_rows = jnp.sin(angles)[:, None, :]
    first_half = field_rows[..., :half_width]
    second = field_rows[..., half_width:]
    return jnp.concatenate(
        [first_half * cosine - second * sine_rows, second * cosine + first_half * sine_rows],
        axis=-1,
    )


def on_device(tokens, query_weight, key_weight, value_weight, output_weight, block_choice):
    features = tokens[0]
    row_count = features.shape[0]
    rank_here = lax.axis_index("kv")
    query_width = query_weight.shape[1]
    key_width = key_weight.shape[1]
    head_count = query_width // HEAD
    kv_count = key_width // HEAD
    group_size = head_count // kv_count
    block_count = row_count // BLOCK
    query_sum = jnp.dot(
        features,
        lax.all_gather(query_weight, "kv", axis=0, tiled=True),
        preferred_element_type=jnp.float32,
    )
    key_sum = jnp.dot(
        features,
        lax.all_gather(key_weight, "kv", axis=0, tiled=True),
        preferred_element_type=jnp.float32,
    )
    value_sum = jnp.dot(
        features,
        lax.all_gather(value_weight, "kv", axis=0, tiled=True),
        preferred_element_type=jnp.float32,
    )
    positions = rank_here * row_count + jnp.arange(row_count, dtype=jnp.int32)
    queries = rotate(query_sum.reshape(row_count, head_count, HEAD), positions).astype(jnp.bfloat16)
    key_rows = rotate(key_sum.reshape(row_count, kv_count, HEAD), positions).astype(jnp.bfloat16)
    value_rows = value_sum.astype(jnp.bfloat16)
    query_blocks = queries.reshape(block_count, BLOCK, kv_count, group_size, HEAD)
    key_blocks = key_rows.reshape(block_count, BLOCK, kv_count, HEAD)
    value_blocks = value_rows.reshape(block_count, BLOCK, kv_count, HEAD)
    listed_ids = block_choice[0]
    listed = listed_ids >= 0
    pool_keys, pool_values = (
        lax.all_gather(key_blocks, "kv", axis=0, tiled=True),
        lax.all_gather(value_blocks, "kv", axis=0, tiled=True),
    )
    pool_index = jnp.maximum(listed_ids, 0)
    span = 2
    turns = block_count // span
    offsets = jnp.arange(BLOCK, dtype=jnp.int32)
    causal = offsets[None, :] <= offsets[:, None]

    def attend(inputs):
        span_queries, span_keys, span_values, span_index, span_listed = inputs
        near_keys = jnp.concatenate(
            [pool_keys[span_index].reshape(span, NSEL * BLOCK, kv_count, HEAD), span_keys], axis=1
        )
        near_values = jnp.concatenate(
            [pool_values[span_index].reshape(span, NSEL * BLOCK, kv_count, HEAD), span_values],
            axis=1,
        )
        listed_keys = jnp.repeat(span_listed, BLOCK, axis=1)
        visible = jnp.concatenate(
            [
                jnp.broadcast_to(listed_keys[:, None, :], (span, BLOCK, NSEL * BLOCK)),
                jnp.broadcast_to(causal[None], (span, BLOCK, BLOCK)),
            ],
            axis=2,
        )
        scores = jnp.einsum(
            "bqgrd,bkgd->bgrqk", span_queries, near_keys, preferred_element_type=jnp.float32
        ) * HEAD ** (-0.5)
        scores = jnp.where(visible[:, None, None], scores, NEGATIVE)
        row_top = jnp.max(scores, axis=-1, keepdims=True)
        weights = jnp.exp(scores - row_top)
        row_total = jnp.sum(weights, axis=-1)
        weighted = jnp.einsum(
            "bgrqk,bkgd->bqgrd",
            weights.astype(jnp.bfloat16),
            near_values,
            preferred_element_type=jnp.float32,
        )
        weighted = weighted / jnp.transpose(row_total, (0, 3, 1, 2))[..., None]
        return weighted.astype(jnp.bfloat16)

    mixed = lax.map(
        attend,
        (
            query_blocks.reshape(turns, span, BLOCK, kv_count, group_size, HEAD),
            key_blocks.reshape(turns, span, BLOCK, kv_count, HEAD),
            value_blocks.reshape(turns, span, BLOCK, kv_count, HEAD),
            pool_index.reshape(turns, span, NSEL),
            listed.reshape(turns, span, NSEL),
        ),
    )
    mixed = mixed.reshape(row_count, query_width)
    piece_out = jnp.dot(
        mixed,
        lax.all_gather(output_weight, "kv", axis=1, tiled=True),
        preferred_element_type=jnp.float32,
    )
    rounded = lax.optimization_barrier(piece_out.astype(jnp.bfloat16)).astype(jnp.float32)
    summed = lax.psum_scatter(rounded.astype(jnp.bfloat16), "tp", scatter_dimension=1, tiled=True)
    return summed[None]


def solution(mesh):
    return jax.shard_map(
        on_device,
        mesh=mesh,
        in_specs=(
            P(("grp", "dp"), "kv", None),
            P("kv", "tp"),
            P("kv", "tp"),
            P("kv", "tp"),
            P("tp", "kv"),
            P(("grp", "dp"), "kv", None),
        ),
        out_specs=P(("grp", "dp"), "kv", "tp"),
        check_vma=False,
    )
```

profile of v0, /device:TPU:25, one launch (start us, length us, event | category | flops | bytes accessed | tf_op | source)
XLA Modules:
  0.0 198.9 jit_solution(1576839863931789407)
XLA Ops:
  11.2 25.0 %all-gather.7.cloned.1.call-done = bf16[2048,256]{1,0:T(8,128)(2,1)} async-done(((bf16[512,256]{1,0:T(8,128)(2,1)}), bf16[2048,256]{1,0:T(8,128)(2,1)}) %all-gather.7.cloned.1.call-update) | async-done | bytes 1048592 | tf_op jit(solution)/shard_map/all_gather | solution.py:46
  36.2 1.5 copy.46
  39.2 26.0 %all-gather.5.cloned.1.call-done = bf16[2048,256]{1,0:T(8,128)(2,1)} async-done(((bf16[512,256]{1,0:T(8,128)(2,1)}), bf16[2048,256]{1,0:T(8,128)(2,1)}) %all-gather.5.cloned.1.call-update) | async-done | bytes 1048592 | tf_op jit(solution)/shard_map/all_gather | solution.py:51
  65.2 1.8 fusion.37
  68.3 24.1 %all_gather.21 = bf16[24,64,2,128]{3,1,2,0:T(8,128)(2,1)S(1)} all-gather(bf16[6,64,2,128]{3,1,2,0:T(8,128)(2,1)S(1)} %pad_maximum_fusion.1), channel_id=1, replica_groups=mesh['grp'=2,'dp'=2,'kv'=4,'tp'=2] {'kv'}, dimensions={0}, use_global_device_ids=true | all-gather | bytes 983040 | tf_op jit(solution)/shard_map/all_gather | solution.py:64
  92.8 28.9 %all_gather.19 = bf16[24,64,2,128]{3,1,2,0:T(8,128)(2,1)} all-gather(bf16[6,64,2,128]{3,1,2,0:T(8,128)(2,1)S(1)} %copy.45), channel_id=1, replica_groups=mesh['grp'=2,'dp'=2,'kv'=4,'tp'=2] {'kv'}, dimensions={0}, use_global_device_ids=true | all-gather | bytes 983040 | tf_op jit(solution)/shard_map/all_gather | solution.py:65
  122.5 9.5 %all-gather.9.cloned.1.call-done = bf16[2048,512]{1,0:T(8,128)(2,1)} async-done(((bf16[512,512]{1,0:T(8,128)(2,1)}), bf16[2048,512]{1,0:T(8,128)(2,1)}) %all-gather.9.cloned.1.call-update) | async-done | bytes 2097168 | tf_op jit(solution)/shard_map/all_gather | solution.py:41
  132.0 4.0 %copy.51 = bf16[512,2048]{1,0:T(8,128)(2,1)} copy(bf16[512,2048]{0,1:T(8,128)(2,1)} %bitcast.106) | data formatting | bytes 4194304 | tf_op jit(solution)/shard_map/dot_general | solution.py:39
  135.9 2.9 %fusion.31 = f32[384,4,128]{0,2,1:T(8,128)S(1)} fusion(bf16[4,128,2048]{2,1,0:T(8,128)(2,1)} %bitcast.107, bf16[1,384,2048]{2,1,0:T(8,128)(2,1)S(1)} %copy-done), kind=kOutput, calls=%fused_computation.38 | convolution fusion | flops 805306368 | bytes 4456448 | tf_op jit(solution)/shard_map/dot_general | solution.py:39
  141.2 34.1 %while.11 = (s32[]{:T(128)}, bf16[3,2,64,2,2,128]{5,4,3,2,1,0:T(2,128)(2,1)}, s32[3,2,16]{2,1,0:T(2,128)S(1)}, bf16[24,64,2,128]{3,1,2,0:T(8,128)(2,1)}, bf16[3,...) while((s32[]{:T(128)}, ...), condition=%wide.region_3.4_spmd.clone, body=%wide.region_0.3_spmd.clone.sunk | while | flops 293843040 | bytes 36634764 | solution.py:106
  142.0 1.1 copy.80
  144.2 1.9 fusion.57
  147.6 1.9 gather_fusion.1
  149.5 1.0 constant_dynamic-slice_fusion.3
  153.4 1.1 copy.80
  155.6 1.9 fusion.57
  158.9 1.9 gather_fusion.1
  164.8 1.1 copy.80
  166.9 1.9 fusion.57
  170.3 1.9 gather_fusion.1
  175.3 1.1 reshape.130
  176.4 1.8 all-gather.11.cloned.1.call-done
  178.2 3.7 %convolution_convert_fusion = bf16[384,2048]{1,0:T(8,128)(2,1)} fusion(bf16[384,512]{1,0:T(8,128)(2,1)S(1)} %reshape.130, bf16[512,2048]{1,0:T(8,128)(2,1)} %all-gather.11.cloned.1.call-done), kind=kOutput, calls=%fused_computation.37 | convolution fusion | flops 806092800 | bytes 4063232 | tf_op jit(solution)/shard_map/dot_general | solution.py:117
  182.0 10.4 %reduce-scatter.2.cloned.1.call-done = bf16[384,1024]{1,0:T(8,128)(2,1)} async-done(((bf16[384,2048]{1,0:T(8,128)(2,1)}), bf16[384,1024]{1,0:T(8,128)(2,1)}) %reduce-scatter.2.cloned.1.call-update) | async-done | bytes 786448 | tf_op jit(solution)/shard_map/reduce_scatter | solution.py:123
  (105 shorter events, 29.1 us)
Async XLA Ops:
  6.5 31.2 %copy-start = (bf16[1,384,2048]{2,1,0:T(8,128)(2,1)S(1)}, bf16[1,384,2048]{2,1,0:T(8,128)(2,1)}, u32[]{:S(2)}) copy-start(bf16[1,384,2048]{2,1,0:T(8,128)(2,1)} %param.8) | copy-start | bytes 4718596
  6.5 29.7 %all-gather.7.cloned.1.call-start = ((), (), s32[]{:S(2)}) async-start(), calls=%async_computation.2 | async-start | bytes 1310720 | tf_op jit(solution)/shard_map/all_gather | solution.py:46
  7.3 57.9 %all-gather.5.cloned.1.call-start = ((), (), s32[]{:S(2)}) async-start(), calls=%async_computation.1 | async-start | bytes 1310720 | tf_op jit(solution)/shard_map/all_gather | solution.py:51
  8.0 124.0 %all-gather.9.cloned.1.call-start = ((), (), s32[]{:S(2)}) async-start(), calls=%async_computation.3 | async-start | bytes 2621440 | tf_op jit(solution)/shard_map/all_gather | solution.py:41
  8.7 169.5 %all-gather.11.cloned.1.call-start = ((), (), s32[]{:S(2)}) async-start(), calls=%async_computation.4 | async-start | bytes 2621440 | tf_op jit(solution)/shard_map/all_gather | solution.py:119
  9.3 183.1 %reduce-scatter.2.cloned.1.call-start = ((), (), s32[]{:S(2)}) async-start(), calls=%async_computation.5 | async-start | bytes 2359296 | tf_op jit(solution)/shard_map/reduce_scatter | solution.py:123
  146.1 1.4 copy-start.1
  149.5 1.7 copy-start.2
  157.5 1.4 copy-start.1
  160.8 1.7 copy-start.2
  168.9 1.4 copy-start.1
  172.2 1.7 copy-start.2
Sparse Core Ops, SparseCore 0:
  8.9 27.2 all-gather.6
  37.8 27.3 all-gather.4
  66.8 65.1 all-gather.8
  133.4 44.8 all-gather.10
  182.1 10.2 reduce-scatter.1
where the time goes:
time: 201 us; the launch traced here: 199 us
  waiting for transfers between devices  75.3 us (37%)
  blocking collectives  52.9 us (26%)
  local copies, waits for them, and re-layouts  34.7 us (17%)
  matrix products  16.6 us (8%)
  between operations  13.3 us (7%)
  other arithmetic  5.59 us (3%)
    all_gather x1, blocking collectives, on_device(): lax.all_gather(value_blocks, 'kv', axis=0, tiled=True)  28.9 us
    all_gather x1, waiting for transfers between devices, on_device(): lax.all_gather(value_weight, 'kv', axis=0, tiled=True)  26 us
    all_gather x1, waiting for transfers between devices, on_device(): lax.all_gather(key_weight, 'kv', axis=0, tiled=True)  25 us
    all_gather x1, blocking collectives, on_device(): lax.all_gather(key_blocks, 'kv', axis=0, tiled=True)  24.1 us
    reduce_scatter x1, waiting for transfers between devices, on_device(): lax.psum_scatter(rounded.astype(jnp.bfloat16), 'tp', scatter_dimension=1,...  10.4 us
    all_gather x1, waiting for transfers between devices, on_device(): lax.all_gather(query_weight, 'kv', axis=0, tiled=True)  9.48 us
    gather x6, local copies, waits for them, and re-layouts, attend(): pool_values[span_index].reshape(span, NSEL * BLOCK, kv_count, HEAD)  5.86 us
    dot_general x3, matrix products, attend(): jnp.einsum('bqgrd,bkgd->bgrqk', span_queries, near_keys, preferred_elemen...  5.8 us
  transfers between devices with their start and end apart: 5, of which 5 were waited for; matrix products, arithmetic and copies ran while one was open for 25% of the time, Pallas kernels for 0%

commit v1 on v0

v1 whole, which is shorter than its diff:
```python
import functools

import jax
import jax.numpy as jnp
from jax import lax
from jax.experimental import pallas as pl
from jax.experimental.pallas import tpu as pltpu
from jax.sharding import PartitionSpec as P

HEAD = 128
BLOCK = 64
THETA = 10000.0
NEGATIVE = -1e30
MESH = pl.DeviceIdType.MESH
QUARTERS = 4


def kernel(n, tokens_hbm, wk_hbm, wv_hbm, wq_hbm, wo_hbm, cos_ref, sin_ref, bias_ref, out_ref,
           tokens, wk_all, wv_all, wq_all, wo_all, kpool, vpool, qbuf, mixed, outgoing, incoming,
           own_sem, z_send, z_recv, xy_send, xy_recv, kv_send, kv_recv, tp_send, tp_recv):
    g, d, z, t = (lax.axis_index(a) for a in ("grp", "dp", "kv", "tp"))
    gx, dx, tx = g + 1 - 2 * (g % 2), d + 1 - 2 * (d % 2), 1 - t
    up, down = jnp.minimum(z + 1, n - 1), jnp.maximum(z - 1, 0)
    up_id, down_id, tp_id = (g, d, up, t), (g, d, down, t), (g, d, z, tx)
    plane = ((g, dx, z, t), (gx, d, z, t), (gx, dx, z, t))
    mine = (g % 2) * 2 + d % 2
    theirs = ((g % 2) * 2 + dx % 2, (gx % 2) * 2 + d % 2, (gx % 2) * 2 + dx % 2)
    rows = tokens.shape[0]
    shards = (wk_hbm, wv_hbm, wq_hbm, wo_hbm)
    gathered = (wk_all, wv_all, wq_all, wo_all)
    depths = tuple(s.shape[0] for s in shards)
    parts = tuple(x // QUARTERS for x in depths)

    def place(w, origin, quarter):
        start = pl.multiple_of(quarter * parts[w], parts[w])
        return gathered[w].at[origin, pl.ds(start, parts[w])]

    def own_copy(w):
        return pltpu.make_async_copy(shards[w], gathered[w].at[z], own_sem.at[w])

    tokens_copy = pltpu.make_async_copy(tokens_hbm, tokens, own_sem.at[4])

    def z_copy(w, origin, way, own=False):
        start = pl.multiple_of(mine * parts[w], parts[w])
        source = shards[w].at[pl.ds(start, parts[w])] if own else place(w, origin, mine)
        return pltpu.make_async_remote_copy(
            src_ref=source, dst_ref=place(w, origin, mine),
            send_sem=z_send.at[w, origin, way], recv_sem=z_recv.at[w, origin],
            device_id=(up_id, down_id)[way], device_id_type=MESH)

    def xy_copy(w, origin, peer, arriving=False):
        where = place(w, origin, theirs[peer] if arriving else mine)
        return pltpu.make_async_remote_copy(
            src_ref=where, dst_ref=where,
            send_sem=xy_send.at[w, origin, peer], recv_sem=xy_recv.at[w, origin, peer],
            device_id=plane[peer], device_id_type=MESH)

    def kv_copy(which, origin):
        pool = (kpool, vpool)[which]
        where = pool.at[pl.ds(pl.multiple_of(origin * rows, rows), rows)]
        return pltpu.make_async_remote_copy(
            src_ref=where, dst_ref=where, send_sem=kv_send.at[which, origin],
            recv_sem=kv_recv.at[which, origin], device_id=up_id, device_id_type=MESH)

    def tp_copy(j):
        return pltpu.make_async_remote_copy(
            src_ref=outgoing.at[j], dst_ref=incoming.at[j], send_sem=tp_send.at[j],
            recv_sem=tp_recv.at[j], device_id=tp_id, device_id_type=MESH)

    def send_own(w):
        @pl.when(z + 1 < n)
        def _():
            z_copy(w, z, 0, True).start()

        @pl.when(z > 0)
        def _():
            z_copy(w, z, 1, True).start()

    def relay(w):
        def step(s, carry):
            @pl.when(z - s >= 0)
            def _():
                origin = z - s
                z_copy(w, origin, 0).wait_recv()
                for peer in range(3):
                    xy_copy(w, origin, peer).start()

                @pl.when(z + 1 < n)
                def _():
                    z_copy(w, origin, 0).start()

            @pl.when(z + s < n)
            def _():
                origin = z + s
                z_copy(w, origin, 1).wait_recv()
                for peer in range(3):
                    xy_copy(w, origin, peer).start()

                @pl.when(z > 0)
                def _():
                    z_copy(w, origin, 1).start()
            return carry
        lax.fori_loop(1, n, step, 0)

    def settle(w):
        own_copy(w).wait()

        def step(s, carry):
            origin = (z + s) % n
            for peer in range(3):
                xy_copy(w, origin, peer, True).wait_recv()
            return carry
        lax.fori_loop(1, n, step, 0)

    def kv_relay(first, last):
        def step(s, carry):
            @pl.when(z - s >= 0)
            def _():
                for which in range(2):
                    kv_copy(which, z - s).wait_recv()

                    @pl.when(z + 1 < n)
                    def _():
                        kv_copy(which, z - s).start()
            return carry
        lax.fori_loop(first, last, step, 0)

    tokens_copy.start()
    for w in range(4):
        own_copy(w).start()

    barrier = pltpu.get_barrier_semaphore()
    for peer in plane + (tp_id,):
        pl.semaphore_signal(barrier, inc=1, device_id=peer, device_id_type=MESH)

    @pl.when(z + 1 < n)
    def _():
        pl.semaphore_signal(barrier, inc=1, device_id=up_id, device_id_type=MESH)

    @pl.when(z > 0)
    def _():
        pl.semaphore_signal(barrier, inc=1, device_id=down_id, device_id_type=MESH)
    pl.semaphore_wait(barrier, 4 + jnp.where(z + 1 < n, 1, 0) + jnp.where(z > 0, 1, 0))

    def project(gathered_ref):
        total = None
        depth = gathered_ref.shape[1]
        for origin in range(n):
            piece = jnp.dot(tokens[:, origin * depth:(origin + 1) * depth], gathered_ref[origin],
                            preferred_element_type=jnp.float32)
            total = piece if total is None else total + piece
        return total

    def turned(total):
        heads = total.shape[1] // HEAD
        out = []
        for h in range(heads):
            u = total[:, h * HEAD:(h + 1) * HEAD]
            out.append(u * cos_ref[...] + pltpu.roll(u, HEAD // 2, 1) * sin_ref[...])
        return jnp.concatenate(out, axis=1).astype(jnp.bfloat16)

    send_own(0)
    send_own(1)
    relay(0)
    send_own(2)
    relay(1)
    send_own(3)
    relay(2)
    tokens_copy.wait()
    here = pl.ds(pl.multiple_of(z * rows, rows), rows)
    def clear(s, carry):
        @pl.when(z + s < n)
        def _():
            past = pl.ds(pl.multiple_of((z + s) * rows, rows), rows)
            kpool[past] = jnp.zeros((rows, kpool.shape[1]), kpool.dtype)
            vpool[past] = jnp.zeros((rows, vpool.shape[1]), vpool.dtype)
        return carry
    lax.fori_loop(1, n, clear, 0)
    settle(0)
    kpool[here] = turned(project(wk_all))
    settle(1)
    vpool[here] = project(wv_all).astype(jnp.bfloat16)

    @pl.when(z + 1 < n)
    def _():
        kv_copy(0, z).start()
        kv_copy(1, z).start()
    relay(3)
    kv_relay(1, min(2, n))
    settle(2)
    qbuf[...] = turned(project(wq_all))
    kv_relay(min(2, n), n)

    kv_heads = kpool.shape[1] // HEAD
    group = qbuf.shape[1] // kpool.shape[1]
    contract = (((1,), (1,)), ((), ()))

    def attend(i, carry):
        at = pl.multiple_of(i * BLOCK, BLOCK)
        near = pl.multiple_of(z * rows + i * BLOCK, BLOCK)
        bias = bias_ref[i]
        row = lax.broadcasted_iota(jnp.int32, (group * BLOCK, BLOCK), 0) % BLOCK
        column = lax.broadcasted_iota(jnp.int32, (group * BLOCK, BLOCK), 1)
        for h in range(kv_heads):
            lanes = slice(h * HEAD, (h + 1) * HEAD)
            q = jnp.concatenate([
                qbuf[pl.ds(at, BLOCK), (h * group + r) * HEAD:(h * group + r + 1) * HEAD]
                for r in range(group)], axis=0)
            far = lax.dot_general(q, kpool[:, lanes], contract,
                                  preferred_element_type=jnp.float32) * HEAD ** (-0.5) + bias
            own = lax.dot_general(q, kpool[pl.ds(near, BLOCK), lanes], contract,
                                  preferred_element_type=jnp.float32) * HEAD ** (-0.5)
            own = jnp.where(column <= row, own, NEGATIVE)
            top = jnp.maximum(jnp.max(far, axis=1, keepdims=True), jnp.max(own, axis=1, keepdims=True))
            far = jnp.exp(far - top)
            own = jnp.exp(own - top)
            total = jnp.sum(far, axis=1, keepdims=True) + jnp.sum(own, axis=1, keepdims=True)
            weighted = jnp.dot(far.astype(jnp.bfloat16), vpool[:, lanes],
                               preferred_element_type=jnp.float32)
            weighted += jnp.dot(own.astype(jnp.bfloat16), vpool[pl.ds(near, BLOCK), lanes],
                                preferred_element_type=jnp.float32)
            weighted = (weighted / total).astype(jnp.bfloat16)
            for r in range(group):
                mixed[pl.ds(at, BLOCK), (h * group + r) * HEAD:(h * group + r + 1) * HEAD] = (
                    weighted[r * BLOCK:(r + 1) * BLOCK])
        return carry
    lax.fori_loop(0, rows // BLOCK, attend, 0)

    settle(3)
    half = n // 2
    width = wo_all.shape[2]
    for j in range(half):
        outgoing[j] = jnp.dot(mixed[...], wo_all[tx * half + j],
                              preferred_element_type=jnp.float32).astype(jnp.bfloat16)
        if j > 0:
            tp_copy(j - 1).start()
    for j in range(half):
        out_ref[:, j * width:(j + 1) * width] = jnp.dot(
            mixed[...], wo_all[t * half + j], preferred_element_type=jnp.float32).astype(jnp.bfloat16)
        if j == 0:
            tp_copy(half - 1).start()
    for j in range(half):
        tp_copy(j).wait_recv()
        columns = slice(j * width, (j + 1) * width)
        out_ref[:, columns] = (out_ref[:, columns].astype(jnp.float32)
                               + incoming[j].astype(jnp.float32)).astype(jnp.bfloat16)

    for j in range(half):
        tp_copy(j).wait_send()

    def drain(origin, carry):
        @pl.when(origin <= z)
        def _():
            @pl.when(z + 1 < n)
            def _():
                for which in range(2):
                    kv_copy(which, origin).wait_send()
                for w in range(4):
                    z_copy(w, origin, 0).wait_send()

        @pl.when(origin >= z)
        def _():
            @pl.when(z > 0)
            def _():
                for w in range(4):
                    z_copy(w, origin, 1).wait_send()

        @pl.when(origin != z)
        def _():
            for w in range(4):
                for peer in range(3):
                    xy_copy(w, origin, peer).wait_send()
        return carry
    lax.fori_loop(0, n, drain, 0)


def on_device(n, tokens, query_weight, key_weight, value_weight, output_weight, block_choice):
    features = tokens[0]
    rows, model = features.shape
    z = lax.axis_index("kv")
    query_width = query_weight.shape[1]
    key_width = key_weight.shape[1]
    blocks = rows // BLOCK
    keys = n * rows
    half_width = HEAD // 2
    positions = z * rows + jnp.arange(rows, dtype=jnp.int32)
    inverse = THETA ** (-jnp.arange(half_width, dtype=jnp.float32) / half_width)
    angles = positions.astype(jnp.float32)[:, None] * inverse[None, :]
    cosine, sine = jnp.cos(angles), jnp.sin(angles)
    cosine = jnp.concatenate([cosine, cosine], axis=1)
    sine = jnp.concatenate([-sine, sine], axis=1)
    named = jnp.any(block_choice[0][:, :, None] == jnp.arange(keys // BLOCK, dtype=jnp.int32), axis=1)
    bias = jnp.repeat(jnp.where(named, 0.0, NEGATIVE).astype(jnp.float32), BLOCK, axis=1)
    bias = bias[:, None, :]
    anywhere = pl.BlockSpec(memory_space=pl.ANY)
    inside = pl.BlockSpec(memory_space=pltpu.VMEM)
    depth = key_weight.shape[0]
    out_rows, out_columns = output_weight.shape
    bf16 = jnp.bfloat16
    dma = pltpu.SemaphoreType.DMA
    out = pl.pallas_call(
        functools.partial(kernel, n),
        out_shape=jax.ShapeDtypeStruct((rows, n * out_columns // 2), bf16),
        in_specs=[anywhere] * 5 + [inside] * 3,
        out_specs=inside,
        scratch_shapes=[
            pltpu.VMEM((rows, model), bf16),
            pltpu.VMEM((n, depth, key_width), bf16),
            pltpu.VMEM((n, depth, key_width), bf16),
            pltpu.VMEM((n, depth, query_width), bf16),
            pltpu.VMEM((n, out_rows, out_columns), bf16),
            pltpu.VMEM((keys, key_width), bf16),
            pltpu.VMEM((keys, key_width), bf16),
            pltpu.VMEM((rows, query_width), bf16),
            pltpu.VMEM((rows, query_width), bf16),
            pltpu.VMEM((n // 2, rows, out_columns), bf16),
            pltpu.VMEM((n // 2, rows, out_columns), bf16),
            dma((5,)), dma((4, n, 2)), dma((4, n)), dma((4, n, 3)), dma((4, n, 3)),
            dma((2, n)), dma((2, n)), dma((n // 2,)), dma((n // 2,)),
        ],
        compiler_params=pltpu.CompilerParams(
            collective_id=0, has_side_effects=True, vmem_limit_bytes=60 * 1024 * 1024),
    )(features, key_weight, value_weight, query_weight, output_weight, cosine, sine, bias)
    return out[None]


def solution(mesh):
    return jax.shard_map(
        functools.partial(on_device, mesh.shape["kv"]),
        mesh=mesh,
        in_specs=(
            P(("grp", "dp"), "kv", None),
            P("kv", "tp"),
            P("kv", "tp"),
            P("kv", "tp"),
            P("tp", "kv"),
            P(("grp", "dp"), "kv", None),
        ),
        out_specs=P(("grp", "dp"), "kv", "tp"),
        check_vma=False,
    )
```

time: 201 us -> 74.9 us (0.37)
  waiting for transfers between devices: 75.3 us -> 0 us
  Pallas kernels: 0 us -> 69.4 us
  blocking collectives: 52.9 us -> 0 us
  local copies, waits for them, and re-layouts: 34.7 us -> 3.56 us
  matrix products: 16.6 us -> 0 us
  between operations: 13.3 us -> 0.03 us
  other arithmetic: 5.59 us -> 1.79 us
    pallas_call x0 -> x1, Pallas kernels: none -> 69.4 us  [on_device(): pl.pallas_call(functools.partial(kernel, n), out_shape=jax.ShapeDtypeStru...]
    all_gather x4 -> x0, waiting for transfers between devices: 62.3 us -> none  [the longest x1 26 us: on_device(): lax.all_gather(value_weight, 'kv', axis=0, tiled=True)]
    all_gather x2 -> x0, blocking collectives: 52.9 us -> none  [the longest x1 28.9 us: on_device(): lax.all_gather(value_blocks, 'kv', axis=0, tiled=True)]
    dot_general x10 -> x0, matrix products: 16.6 us -> none  [the longest x3 5.8 us: attend(): jnp.einsum('bqgrd,bkgd->bgrqk', span_queries, near_keys, preferred_elemen...]
    gather x12 -> x0, local copies, waits for them, and re-layouts: 11.3 us -> none  [the longest x6 5.86 us: attend(): pool_values[span_index].reshape(span, NSEL * BLOCK, kv_count, HEAD)]
    reduce_scatter x1 -> x0, waiting for transfers between devices: 10.4 us -> none  [on_device(): lax.psum_scatter(rounded.astype(jnp.bfloat16), 'tp', scatter_dimension=1,...]
    dot_general x2 -> x0, local copies, waits for them, and re-layouts: 5.44 us -> none  [the longest x1 3.96 us: on_device(): jnp.dot(features, lax.all_gather(query_weight, 'kv', axis=0, tiled=True),...]
    while x12 -> x0, local copies, waits for them, and re-layouts: 4.34 us -> none
  transfers between devices with their start and end apart: 5 -> 0, of which waited for: 5 -> 0; matrix products, arithmetic and copies ran while one was open for 25% -> 0% of each run, Pallas kernels for 0% -> 0%
where the time goes in v1:
time: 74.9 us; the launch traced here: 74.8 us
  Pallas kernels  69.4 us (93%)
  local copies, waits for them, and re-layouts  3.56 us (5%)
  other arithmetic  1.79 us (2%)
    pallas_call x1, Pallas kernels, on_device(): pl.pallas_call(functools.partial(kernel, n), out_shape=jax.ShapeDtypeStru...  69.4 us
    unnamed x2, local copies, waits for them, and re-layouts  2.75 us

profile of v1, /device:TPU:25, one launch (start us, length us, event | category | flops | bytes accessed | tf_op | source)
XLA Modules:
  0.0 74.8 jit_solution(13199833961592339047)
XLA Ops:
  0.0 0.7 copy.9
  0.7 0.1 fusion.1
  0.8 0.1 broadcast_in_dim.19
  0.9 0.7 broadcast_in_dim_reshape.3.bias_ref
  1.6 0.8 %fusion = (f32[384,64]{1,0:T(8,128)S(1)}, f32[384,64]{1,0:T(8,128)S(1)}, f32[384,64]{1,0:T(8,128)S(1)}) fusion(f32[64]{0:T(128)S(1)} %multiply_power_fusion, f32[384]{0:T(512)S(1)} %add_convert_fusion), kind=kLoop, calls=%fused_computation.4 | loop fusion | flops 49152 | bytes 296704 | tf_op jit(solution)/shard_map/neg | solution.py:291
  2.4 0.9 %pad_maximum_fusion = (f32[384,128]{1,0:T(8,128)}, f32[384,128]{1,0:T(8,128)}) fusion(f32[384,64]{1,0:T(8,128)S(1)} %get-tuple-element.7, f32[384,64]{1,0:T(8,128)S(1)} %get-tuple-element.6, f32[384,64]{1,0:T(8,128)S(1)} %get-tuple-element.5), kind=kLoop, calls=%fused_computation.2 | loop fusion | flops 98304 | bytes 688128 | tf_op jit(solution)/shard_map/concatenate | solution.py:290
  3.3 69.4 %shard_map.64 = bf16[384,1024]{1,0:T(8,128)(2,1)} custom-call(bf16[384,2048]{1,0:T(8,128)(2,1)} %bitcast.6, bf16[512,256]{1,0:T(8,128)(2,1)} %wk_hbm.1, bf16[512,256]{1,0:T(8,128)(2,1)} %wv_hbm.1, bf16[512,512]{1,0:T(8,128)(2,1)} %wq_hbm.1, bf16[512,512]{1,0:T(8,128)(2,1)} %wo_hbm.1, f32[384,128]{1,0:T(8,128)} %get-tuple-element.8.cos_ref, ...), custom_call_target="tpu_custom_call" | custom-call | tf_op jit(solution)/shard_map/pallas_call | solution.py:301
  72.7 2.1 %copy.11 = bf16[1,384,1024]{2,1,0:T(8,128)(2,1)} copy(bf16[1,384,1024]{2,1,0:T(8,128)(2,1)} %bitcast.5) | data formatting | bytes 1572864
  (3 shorter events, 0.0 us)

commit v2 on v1

--- a/solution.py
+++ b/solution.py
@@ -1,6 +1,7 @@
 import functools
 
 import jax
+import numpy as np
 import jax.numpy as jnp
 from jax import lax
 from jax.experimental import pallas as pl
@@ -15,8 +16,8 @@
 QUARTERS = 4
 
 
-def kernel(n, tokens_hbm, wk_hbm, wv_hbm, wq_hbm, wo_hbm, cos_ref, sin_ref, bias_ref, out_ref,
-           tokens, wk_all, wv_all, wq_all, wo_all, kpool, vpool, qbuf, mixed, outgoing, incoming,
+def kernel(n, tokens_hbm, wk_hbm, wv_hbm, wq_hbm, wo_hbm, choice_ref, frequency_ref, out_ref,
+           tokens, wk_all, wv_all, wq_all, wo_all, kpool, vpool, qbuf, mixed, outgoing, incoming, kept, cosine, sine,
            own_sem, z_send, z_recv, xy_send, xy_recv, kv_send, kv_recv, tp_send, tp_recv):
     g, d, z, t = (lax.axis_index(a) for a in ("grp", "dp", "kv", "tp"))
     gx, dx, tx = g + 1 - 2 * (g % 2), d + 1 - 2 * (d % 2), 1 - t
@@ -26,6 +27,7 @@
     mine = (g % 2) * 2 + d % 2
     theirs = ((g % 2) * 2 + dx % 2, (gx % 2) * 2 + d % 2, (gx % 2) * 2 + dx % 2)
     rows = tokens.shape[0]
+    half = n // 2
     shards = (wk_hbm, wv_hbm, wq_hbm, wo_hbm)
     gathered = (wk_all, wv_all, wq_all, wo_all)
     depths = tuple(s.shape[0] for s in shards)
@@ -38,7 +40,7 @@
     def own_copy(w):
         return pltpu.make_async_copy(shards[w], gathered[w].at[z], own_sem.at[w])
 
-    tokens_copy = pltpu.make_async_copy(tokens_hbm, tokens, own_sem.at[4])
+    tokens_copy = pltpu.make_async_copy(tokens_hbm.at[0], tokens, own_sem.at[4])
 
     def z_copy(w, origin, way, own=False):
         start = pl.multiple_of(mine * parts[w], parts[w])
@@ -76,7 +78,7 @@
         def _():
             z_copy(w, z, 1, True).start()
 
-    def relay(w):
+    def relay(w, first=1, last=n):
         def step(s, carry):
             @pl.when(z - s >= 0)
             def _():
@@ -100,7 +102,7 @@
                 def _():
                     z_copy(w, origin, 1).start()
             return carry
-        lax.fori_loop(1, n, step, 0)
+        lax.fori_loop(first, last, step, 0)
 
     def settle(w):
         own_copy(w).wait()
@@ -156,16 +158,22 @@
         out = []
         for h in range(heads):
             u = total[:, h * HEAD:(h + 1) * HEAD]
-            out.append(u * cos_ref[...] + pltpu.roll(u, HEAD // 2, 1) * sin_ref[...])
+            out.append(u * cosine[...] + pltpu.roll(u, HEAD // 2, 1) * sine[...])
         return jnp.concatenate(out, axis=1).astype(jnp.bfloat16)
 
     send_own(0)
     send_own(1)
+    spot = z * rows + lax.broadcasted_iota(jnp.int32, cosine.shape, 0)
+    angle = spot.astype(jnp.float32) * frequency_ref[...]
+    lane = lax.broadcasted_iota(jnp.int32, cosine.shape, 1)
+    cosine[...] = jnp.cos(angle)
+    sine[...] = jnp.sin(angle) * jnp.where(lane < HEAD // 2, -1.0, 1.0)
     relay(0)
     send_own(2)
     relay(1)
     send_own(3)
     relay(2)
+    relay(3, 1, half)
     tokens_copy.wait()
     here = pl.ds(pl.multiple_of(z * rows, rows), rows)
     def clear(s, carry):
@@ -185,7 +193,7 @@
     def _():
         kv_copy(0, z).start()
         kv_copy(1, z).start()
-    relay(3)
+    relay(3, half, n)
     kv_relay(1, min(2, n))
     settle(2)
     qbuf[...] = turned(project(wq_all))
@@ -198,7 +206,12 @@
     def attend(i, carry):
         at = pl.multiple_of(i * BLOCK, BLOCK)
         near = pl.multiple_of(z * rows + i * BLOCK, BLOCK)
-        bias = bias_ref[i]
+        named = None
+        block = lax.broadcasted_iota(jnp.int32, (1, kpool.shape[0]), 1) // BLOCK
+        for slot in range(choice_ref.shape[2]):
+            match = block == choice_ref[0, i, slot]
+            named = match if named is None else named | match
+        bias = jnp.where(named, 0.0, NEGATIVE)
         row = lax.broadcasted_iota(jnp.int32, (group * BLOCK, BLOCK), 0) % BLOCK
         column = lax.broadcasted_iota(jnp.int32, (group * BLOCK, BLOCK), 1)
         for h in range(kv_heads):
@@ -226,24 +239,39 @@
         return carry
     lax.fori_loop(0, rows // BLOCK, attend, 0)
 
-    settle(3)
-    half = n // 2
+    own_copy(3).wait()
     width = wo_all.shape[2]
-    for j in range(half):
-        outgoing[j] = jnp.dot(mixed[...], wo_all[tx * half + j],
-                              preferred_element_type=jnp.float32).astype(jnp.bfloat16)
-        if j > 0:
-            tp_copy(j - 1).start()
-    for j in range(half):
-        out_ref[:, j * width:(j + 1) * width] = jnp.dot(
-            mixed[...], wo_all[t * half + j], preferred_element_type=jnp.float32).astype(jnp.bfloat16)
-        if j == 0:
-            tp_copy(half - 1).start()
+
+    def finish(origin):
+        piece = jnp.dot(mixed[...], wo_all[origin],
+                        preferred_element_type=jnp.float32).astype(jnp.bfloat16)
+        slot = origin % half
+
+        @pl.when(origin // half == tx)
+        def _():
+            outgoing[slot] = piece
+            tp_copy(slot).start()
+
+        @pl.when(origin // half == t)
+        def _():
+            kept[slot] = piece
+
+    finish(z)
+
+    def collect(s, carry):
+        for origin, there in ((z - s, z - s >= 0), (z + s, z + s < n)):
+            @pl.when(there)
+            def _():
+                for peer in range(3):
+                    xy_copy(3, origin, peer, True).wait_recv()
+                finish(origin)
+        return carry
+    lax.fori_loop(1, n, collect, 0)
     for j in range(half):
         tp_copy(j).wait_recv()
         columns = slice(j * width, (j + 1) * width)
-        out_ref[:, columns] = (out_ref[:, columns].astype(jnp.float32)
-                               + incoming[j].astype(jnp.float32)).astype(jnp.bfloat16)
+        out_ref[0, :, columns] = (kept[j].astype(jnp.float32)
+                                  + incoming[j].astype(jnp.float32)).astype(jnp.bfloat16)
 
     for j in range(half):
         tp_copy(j).wait_send()
@@ -275,23 +303,13 @@
 
 
 def on_device(n, tokens, query_weight, key_weight, value_weight, output_weight, block_choice):
-    features = tokens[0]
-    rows, model = features.shape
-    z = lax.axis_index("kv")
+    rows, model = tokens.shape[1:]
     query_width = query_weight.shape[1]
     key_width = key_weight.shape[1]
-    blocks = rows // BLOCK
     keys = n * rows
     half_width = HEAD // 2
-    positions = z * rows + jnp.arange(rows, dtype=jnp.int32)
-    inverse = THETA ** (-jnp.arange(half_width, dtype=jnp.float32) / half_width)
-    angles = positions.astype(jnp.float32)[:, None] * inverse[None, :]
-    cosine, sine = jnp.cos(angles), jnp.sin(angles)
-    cosine = jnp.concatenate([cosine, cosine], axis=1)
-    sine = jnp.concatenate([-sine, sine], axis=1)
-    named = jnp.any(block_choice[0][:, :, None] == jnp.arange(keys // BLOCK, dtype=jnp.int32), axis=1)
-    bias = jnp.repeat(jnp.where(named, 0.0, NEGATIVE).astype(jnp.float32), BLOCK, axis=1)
-    bias = bias[:, None, :]
+    inverse = (THETA ** (-np.arange(half_width) / half_width)).astype(np.float32)
+    frequency = np.concatenate([inverse, inverse])[None]
     anywhere = pl.BlockSpec(memory_space=pl.ANY)
     inside = pl.BlockSpec(memory_space=pltpu.VMEM)
     depth = key_weight.shape[0]
@@ -300,8 +318,8 @@
     dma = pltpu.SemaphoreType.DMA
     out = pl.pallas_call(
         functools.partial(kernel, n),
-        out_shape=jax.ShapeDtypeStruct((rows, n * out_columns // 2), bf16),
-        in_specs=[anywhere] * 5 + [inside] * 3,
+        out_shape=jax.ShapeDtypeStruct((1, rows, n * out_columns // 2), bf16),
+        in_specs=[anywhere] * 5 + [pl.BlockSpec(memory_space=pltpu.SMEM), inside],
         out_specs=inside,
         scratch_shapes=[
             pltpu.VMEM((rows, model), bf16),
@@ -315,13 +333,16 @@
             pltpu.VMEM((rows, query_width), bf16),
             pltpu.VMEM((n // 2, rows, out_columns), bf16),
             pltpu.VMEM((n // 2, rows, out_columns), bf16),
+            pltpu.VMEM((n // 2, rows, out_columns), bf16),
+            pltpu.VMEM((rows, HEAD), jnp.float32),
+            pltpu.VMEM((rows, HEAD), jnp.float32),
             dma((5,)), dma((4, n, 2)), dma((4, n)), dma((4, n, 3)), dma((4, n, 3)),
             dma((2, n)), dma((2, n)), dma((n // 2,)), dma((n // 2,)),
         ],
         compiler_params=pltpu.CompilerParams(
             collective_id=0, has_side_effects=True, vmem_limit_bytes=60 * 1024 * 1024),
-    )(features, key_weight, value_weight, query_weight, output_weight, cosine, sine, bias)
-    return out[None]
+    )(tokens, key_weight, value_weight, query_weight, output_weight, block_choice, frequency)
+    return out
 
 
 def solution(mesh):

time: 74.9 us -> 72.7 us (0.971)
  other arithmetic: 1.79 us -> 0 us
    concatenate x1 -> x0, other arithmetic: 0.91 us -> none  [on_device(): cosine = jnp.concatenate([cosine, cosine], axis=1)]
    neg x1 -> x0, other arithmetic: 0.76 us -> none  [on_device(): sine = jnp.concatenate([-sine, sine], axis=1)]
where the time goes in v2:
time: 72.7 us; the launch traced here: 72.5 us
  Pallas kernels  69.2 us (95%)
  local copies, waits for them, and re-layouts  3.34 us (5%)
    pallas_call x1, Pallas kernels, on_device(): pl.pallas_call(functools.partial(kernel, n), out_shape=jax.ShapeDtypeStru...  69.2 us
    unnamed x2, local copies, waits for them, and re-layouts  3.34 us

profile of v2, /device:TPU:25, one launch (start us, length us, event | category | flops | bytes accessed | tf_op | source)
XLA Modules:
  0.0 72.5 jit_solution(3730772073542685623)
XLA Ops:
  0.0 1.3 %copy.8.choice_ref = s32[1,6,16]{2,1,0:T(8,128)} copy(s32[1,6,16]{2,0,1:T(1,128)} %param.12) | data formatting | bytes 768 | tf_op args[5]
  1.3 69.2 %shard_map.73 = bf16[1,384,1024]{2,1,0:T(8,128)(2,1)} custom-call(bf16[1,384,2048]{2,1,0:T(8,128)(2,1)} %tokens_hbm.1, bf16[512,256]{1,0:T(8,128)(2,1)} %wk_hbm.1, bf16[512,256]{1,0:T(8,128)(2,1)} %wv_hbm.1, bf16[512,512]{1,0:T(8,128)(2,1)} %wq_hbm.1, bf16[512,512]{1,0:T(8,128)(2,1)} %wo_hbm.1, s32[1,6,16]{2,1,0:T(8,128)} %copy.8.choice_ref, ...), custom_call_target="tpu_custom_call" | custom-call | tf_op jit(solution)/shard_map/pallas_call | solution.py:319
  70.4 2.1 %copy.10 = bf16[1,384,1024]{2,1,0:T(8,128)(2,1)} copy(bf16[1,384,1024]{2,1,0:T(8,128)(2,1)} %shard_map.73) | data formatting | bytes 1572864
